TPU v7x, 32 devices: a whole 2x2x4 slice. The times are simulated.
32 devices in a mesh: ep: 8 (over z, y), tp: 4 (over x, core).
Axes of the slice: x: 2, y: 2, z: 4, core: 2. Of those that a mesh axis runs over, the one named last changes fastest.
Arguments:
- queries: bfloat16 [4096, 1536], P('ep', 'tp'), may hold values from -6 to 6
- keys: bfloat16 [4096, 1536], P('ep', 'tp'), may hold values from -6 to 6
- values: bfloat16 [4096, 1536], P('ep', 'tp'), may hold values from -6 to 6
- decay_gate_logits: float32 [4096, 12], P('ep', 'tp'), may hold values from -6 to 6
- correction_logits: bfloat16 [4096, 12], P('ep', 'tp'), may hold values from -6 to 6
- head_decay_speed: float32 [12], P('tp'), may hold values from 0 to 1
- position_log_decay: float32 [4096, 12], P('ep', 'tp'), may hold values from -1 to 0
- head_output_gain: float32 [128], replicated, may hold values from 0.1 to 1.9
- mixer_output_weight: bfloat16 [1536, 2048], P('tp'), may hold values from -0.15625 to 0.15625
- expert_input_tokens: bfloat16 [4096, 2048], P(('ep', 'tp')), may hold values from -6 to 6
- expert_norm_gain: float32 [2048], replicated, may hold values from 0.1 to 1.9
- routes: int32 [4096, 2], P(('ep', 'tp')), may hold values from 0 to 7, all different within a row; in each aligned block of 128 rows (0 to 127, 128 to 255, ...) at most 48 rows name the same one
- chosen_expert_weight: float32 [4096, 2], P(('ep', 'tp')), may hold values from 0.25 to 2.5
- routed_gate_weight: bfloat16 [8, 2048, 1024], P('ep', None, 'tp'), may hold values from -0.125 to 0.125
- routed_up_weight: bfloat16 [8, 2048, 1024], P('ep', None, 'tp'), may hold values from -0.125 to 0.125
- routed_down_weight: bfloat16 [8, 1024, 2048], P('ep', 'tp'), may hold values from -0.1875 to 0.1875
- common_gate_weight: bfloat16 [2048, 1024], P(None, 'tp'), may hold values from -0.125 to 0.125
- common_up_weight: bfloat16 [2048, 1024], P(None, 'tp'), may hold values from -0.125 to 0.125
- common_down_weight: bfloat16 [1024, 2048], P('tp'), may hold values from -0.1875 to 0.1875
Outputs:
- mixer_out: bfloat16 [4096, 2048], P(('ep', 'tp'))
- moe_out: bfloat16 [4096, 2048], P(('ep', 'tp'))
Inputs may be any that keep to these rules, and one draw needn't show every extreme that they name: `routes`: each row names 2 different experts; the rows of one device name no expert more than 48 times, and some device names some expert exactly 48 times.
All inputs are finite; a program needn't handle non-finite values.
Results may differ from a plain program's by a relative error of at most 0.017.
Values may be sent and summed in bfloat16 or wider, within the bound.
A program may use at most 128 MiB of HBM per device.

v0:
```python
import jax
import jax.numpy as jnp
from jax import lax
from jax.sharding import PartitionSpec as P

EPS = 1e-06
HIGH = lax.Precision.HIGHEST


def prefix_2(x, axis, join, neutral):
    place = lax.axis_index(axis)
    gathered = jax.tree.map(
        lambda a, kind: lax.all_gather(a.astype(kind), axis), x, (jnp.bfloat16, jnp.bfloat16)
    )
    state = jax.tree.map(lambda a, e: jnp.zeros_like(a) + jnp.asarray(e, a.dtype), x, neutral)

    def one(turn, state):
        return join(
            state,
            jax.tree.map(
                lambda a, own: lax.dynamic_index_in_dim(a, turn, 0, False).astype(own.dtype),
                gathered,
                x,
            ),
        )

    return lax.fori_loop(0, place, one, state)


def separate_heads(source, number_of_heads):
    row_count = source.shape[0]
    span_len = 64
    shaped = source.astype(jnp.float32).reshape(
        row_count // span_len, span_len, number_of_heads, source.shape[1] // number_of_heads
    )
    return jnp.transpose(shaped, (2, 0, 1, 3))


def block_contributions(
    queries,
    keys,
    values,
    decay_gate_logits,
    correction_logits,
    head_decay_speed,
    position_log_decay,
):
    number_of_heads = decay_gate_logits.shape[1]
    q_heads = separate_heads(queries, number_of_heads)
    k_heads = separate_heads(keys, number_of_heads)
    v_heads = separate_heads(values, number_of_heads)
    q_heads = (
        q_heads
        * lax.rsqrt(jnp.sum(q_heads * q_heads, axis=-1, keepdims=True) + EPS)
        * q_heads.shape[-1] ** (-0.5)
    )
    k_heads = k_heads * lax.rsqrt(jnp.sum(k_heads * k_heads, axis=-1, keepdims=True) + EPS)
    decay_speed_column = head_decay_speed[:, None, None]
    log_gate_value = (
        -decay_speed_column
        * jax.nn.softplus(separate_heads(decay_gate_logits, number_of_heads)[..., 0])
        + separate_heads(position_log_decay, number_of_heads)[..., 0]
    )
    beta_gate = jax.nn.sigmoid(separate_heads(correction_logits, number_of_heads)[..., 0])
    cum_gate = jnp.cumsum(log_gate_value, axis=-1)
    positions = jnp.arange(log_gate_value.shape[-1])
    causal = positions[:, None] >= positions[None, :]
    strict = positions[:, None] > positions[None, :]
    decay_mat = jnp.exp(
        jnp.where(causal, cum_gate[..., :, None] - cum_gate[..., None, :], -jnp.inf)
    )
    keyed = k_heads * beta_gate[..., None]
    lower_part = jnp.where(
        strict, jnp.einsum("hnld,hnsd->hnls", keyed, k_heads, precision=HIGH) * decay_mat, 0.0
    )
    right_side = jnp.concatenate(
        [v_heads * beta_gate[..., None], keyed * jnp.exp(cum_gate)[..., None]], axis=-1
    )
    solved = lax.linalg.triangular_solve(
        lower_part, right_side, left_side=True, lower=True, unit_diagonal=True
    )
    value_width = v_heads.shape[-1]
    new_values = solved[..., :value_width]
    corr_weights = solved[..., value_width:]
    scores = jnp.einsum("hnld,hnsd->hnls", q_heads, k_heads, precision=HIGH) * decay_mat
    carried_keys = k_heads * jnp.exp(cum_gate[..., -1:] - cum_gate)[..., None]
    q_scaled = q_heads * jnp.exp(cum_gate)[..., None]
    return (q_scaled, cum_gate[..., -1], scores, new_values, corr_weights, carried_keys)


def advance(state, inputs):
    q_blk, last_blk, score_blk, value_blk, weight_blk, carry_blk = inputs
    corrected = value_blk - jnp.einsum("hld,hde->hle", weight_blk, state, precision=HIGH)
    output = jnp.einsum("hld,hde->hle", q_blk, state, precision=HIGH) + jnp.einsum(
        "hls,hse->hle", score_blk, corrected, precision=HIGH
    )
    state = state * jnp.exp(last_blk)[:, None, None] + jnp.einsum(
        "hld,hle->hde", carry_blk, corrected, precision=HIGH
    )
    return (state, output)


def finish_heads(outputs, head_output_gain):
    normed = (
        outputs
        * lax.rsqrt(jnp.mean(outputs * outputs, axis=-1, keepdims=True) + EPS)
        * head_output_gain
    )
    block_count, number_of_heads, span_len, value_width = normed.shape
    normed = jnp.transpose(normed, (0, 2, 1, 3)).reshape(
        block_count * span_len, number_of_heads * value_width
    )
    return normed.astype(jnp.bfloat16)


def mat_product(left_mat, right_mat):
    return jnp.einsum("hde,hef->hdf", left_mat, right_mat, precision=HIGH)


def token_mixer_heads(
    queries,
    keys,
    values,
    decay_gate_logits,
    correction_logits,
    head_decay_speed,
    position_log_decay,
    head_output_gain,
):
    summands = block_contributions(
        queries,
        keys,
        values,
        decay_gate_logits,
        correction_logits,
        head_decay_speed,
        position_log_decay,
    )
    q_scaled, last_gate, scores, new_values, corr_weights, carried_keys = summands
    number_of_heads = q_scaled.shape[0]
    key_width = q_scaled.shape[-1]
    value_width = new_values.shape[-1]
    identity = jnp.broadcast_to(
        jnp.eye(key_width, dtype=jnp.float32), (number_of_heads, key_width, key_width)
    )
    zero_state = jnp.zeros((number_of_heads, key_width, value_width), jnp.float32)
    block_trans = jnp.exp(last_gate)[..., None, None] * jnp.eye(
        key_width, dtype=jnp.float32
    ) - jnp.einsum("hnld,hnle->hnde", carried_keys, corr_weights, precision=HIGH)
    inject = jnp.einsum("hnld,hnle->hnde", carried_keys, new_values, precision=HIGH)

    def compose(state, inputs):
        trans_blk, inject_blk = inputs
        return (
            (mat_product(trans_blk, state[0]), mat_product(trans_blk, state[1]) + inject_blk),
            None,
        )

    (total_trans, total_inject), _ = lax.scan(
        compose,
        (identity, zero_state),
        (jnp.moveaxis(block_trans, 1, 0), jnp.moveaxis(inject, 1, 0)),
    )

    def combine(earlier, later):
        return (mat_product(later[0], earlier[0]), mat_product(later[0], earlier[1]) + later[1])

    prefix = prefix_2((total_trans, total_inject), "ep", combine, (identity, zero_state))
    inputs = tuple((jnp.moveaxis(item, 1, 0) for item in summands))
    _, outputs = lax.scan(advance, prefix[1], inputs)
    return finish_heads(outputs, head_output_gain)


def norm_rows(expert_input_tokens, expert_norm_gain):
    rows_f = expert_input_tokens.astype(jnp.float32)
    scaled = (
        rows_f
        * lax.rsqrt(jnp.mean(rows_f * rows_f, axis=-1, keepdims=True) + EPS)
        * expert_norm_gain
    )
    return scaled.astype(jnp.bfloat16)


def gated_hidden(rows_in, w_gate, w_up):
    gate_val = jnp.dot(rows_in, w_gate, preferred_element_type=jnp.float32)
    up_val = jnp.dot(rows_in, w_up, preferred_element_type=jnp.float32)
    return (jax.nn.silu(gate_val) * up_val).astype(jnp.bfloat16)


def mix_routes(chosen_expert_weight, copies, shared):
    running = shared
    for slot_k in range(chosen_expert_weight.shape[1]):
        running = running + chosen_expert_weight[:, slot_k : slot_k + 1] * copies[:, slot_k].astype(
            jnp.float32
        )
    return running.astype(jnp.bfloat16)


def slot_layout(flat_routes, experts, capacity):
    copy_count = flat_routes.shape[0]
    onehot = (flat_routes[:, None] == jnp.arange(experts, dtype=jnp.int32)[None, :]).astype(
        jnp.int32
    )
    before = jnp.sum(jnp.cumsum(onehot, axis=0) * onehot, axis=1) - 1
    slot_ids = flat_routes * capacity + before
    owners = (
        jnp.full((experts * capacity,), -1, jnp.int32)
        .at[slot_ids]
        .set(jnp.arange(copy_count, dtype=jnp.int32))
    )
    return (slot_ids, owners)


def fill_slots(source_rows, owners, top_k):
    filled = owners >= 0
    source = jnp.where(filled, owners // top_k, 0)
    return jnp.where(filled[:, None], source_rows[source], jnp.zeros((), jnp.bfloat16))


def shards(
    queries,
    keys,
    values,
    decay_gate_logits,
    correction_logits,
    head_decay_speed,
    position_log_decay,
    head_output_gain,
    mixer_output_weight,
    expert_input_tokens,
    expert_norm_gain,
    routes,
    chosen_expert_weight,
    routed_gate_weight,
    routed_up_weight,
    routed_down_weight,
    common_gate_weight,
    common_up_weight,
    common_down_weight,
):
    normed = token_mixer_heads(
        queries,
        keys,
        values,
        decay_gate_logits,
        correction_logits,
        head_decay_speed,
        position_log_decay,
        head_output_gain,
    )
    mixer_out = lax.psum_scatter(
        jnp.dot(normed, mixer_output_weight, preferred_element_type=jnp.float32).astype(
            jnp.bfloat16
        ),
        "tp",
        scatter_dimension=0,
        tiled=True,
    )
    normed_in = norm_rows(expert_input_tokens, expert_norm_gain)
    tokens_own, top_k = routes.shape
    model_width = expert_input_tokens.shape[1]
    experts = lax.axis_size("ep")
    capacity = 3 * tokens_own * top_k // (2 * experts)
    slot_ids, owners = slot_layout(routes.reshape(-1), experts, capacity)
    outgoing = fill_slots(normed_in, owners, top_k).reshape(experts, capacity, model_width)
    arrived = lax.all_to_all(outgoing, "ep", split_axis=0, concat_axis=0, tiled=True).reshape(
        experts * capacity, model_width
    )
    hidden = gated_hidden(
        lax.all_gather(arrived, "tp", axis=0, tiled=True),
        routed_gate_weight[0],
        routed_up_weight[0],
    )
    slot_sums = lax.psum_scatter(
        jnp.dot(hidden, routed_down_weight[0], preferred_element_type=jnp.float32).astype(
            jnp.bfloat16
        ),
        "tp",
        scatter_dimension=0,
        tiled=True,
    )
    returned = lax.all_to_all(
        slot_sums.reshape(experts, capacity, model_width),
        "ep",
        split_axis=0,
        concat_axis=0,
        tiled=True,
    )
    expert_out = returned.reshape(experts * capacity, model_width)[slot_ids]
    shared_hidden = gated_hidden(
        lax.all_gather(normed_in, "tp", axis=0, tiled=True), common_gate_weight, common_up_weight
    )
    shared = lax.psum_scatter(
        jnp.dot(shared_hidden, common_down_weight, preferred_element_type=jnp.float32).astype(
            jnp.bfloat16
        ),
        "tp",
        scatter_dimension=0,
        tiled=True,
    ).astype(jnp.float32)
    moe_out = mix_routes(
        chosen_expert_weight, expert_out.reshape(tokens_own, top_k, model_width), shared
    )
    return (mixer_out, moe_out)


def solution(mesh):
    return jax.shard_map(
        shards,
        mesh=mesh,
        in_specs=(
            P("ep", "tp"),
            P("ep", "tp"),
            P("ep", "tp"),
            P("ep", "tp"),
            P("ep", "tp"),
            P("tp"),
            P("ep", "tp"),
            P(),
            P("tp", None),
            P(("ep", "tp"), None),
            P(),
            P(("ep", "tp"), None),
            P(("ep", "tp"), None),
            P("ep", None, "tp"),
            P("ep", None, "tp"),
            P("ep", "tp", None),
            P(None, "tp"),
            P(None, "tp"),
            P("tp", None),
        ),
        out_specs=(P(("ep", "tp"), None), P(("ep", "tp"), None)),
        check_vma=False,
    )
```

profile of v0, /device:TPU:0, one launch (start us, length us, event | category | flops | bytes accessed | tf_op | source)
XLA Modules:
  0.0 483.4 jit_solution(8555289437563321730)
XLA Ops:
  10.9 1.4 scatter_custom_fusion
  12.3 1.2 fusion.43
  13.6 1.2 fusion.45
  14.9 3.2 gather_fusion
  18.1 1.6 broadcast_select_fusion
  19.6 44.2 %all_to_all.10 = bf16[8,48,2048]{2,1,0:T(8,128)(2,1)} all-to-all(bf16[8,48,2048]{2,1,0:T(8,128)(2,1)S(1)} %broadcast_select_fusion), channel_id=1, replica_groups=mesh['ep'=8,'tp'=4] {'ep'}, dimensions={0} | all-to-all | bytes 3145728 | tf_op jit(solution)/shard_map/all_to_all | solution.py:266
  64.7 44.7 %all-gather.7.cloned.1.call-done = bf16[1536,2048]{1,0:T(8,128)(2,1)} async-done(((bf16[384,2048]{1,0:T(8,128)(2,1)}), bf16[1536,2048]{1,0:T(8,128)(2,1)}) %all-gather.7.cloned.1.call-update) | async-done | bytes 6291472 | tf_op jit(solution)/shard_map/all_gather | solution.py:270
  109.4 5.7 %fusion.52 = f32[1536,256]{1,0:T(8,128)} fusion(bf16[1536,2048]{1,0:T(8,128)(2,1)} %all-gather.7.cloned.1.call-done, bf16[1,2048,256]{2,1,0:T(8,128)(2,1)S(1)} %copy-done.18), kind=kOutput, calls=%fused_computation.75 | convolution fusion | flops 1610612736 | bytes 8912896 | tf_op jit(solution)/shard_map/dot_general | solution.py:185
  115.2 13.2 %convolution_convert_fusion = bf16[1536,2048]{1,0:T(8,128)(2,1)} fusion(bf16[1536,2048]{1,0:T(8,128)(2,1)} %all-gather.7.cloned.1.call-done, f32[1536,256]{1,0:T(8,128)} %fusion.52, bf16[1,256,2048]{2,1,0:T(8,128)(2,1)} %param.40, bf16[1,2048,256]{2,1,0:T(8,128)(2,1)} %param.39), kind=kOutput, calls=%fused_computation.40 | convolution fusion | flops 3226730496 | bytes 16252928 | tf_op jit(solution)/shard_map/dot_general | solution.py:275
  129.9 2.3 reshape.196
  133.6 2.9 fusion.40
  136.6 119.3 %custom-call.3 = f32[3,8,1,64,64]{3,4,2,1,0:T(8,128)} custom-call(f32[3,8,1,64,64]{4,3,2,1,0:T(8,128)} %fusion.40), custom_call_target="InvertDiagBlocksLowerTriangular" | custom-call | tf_op jit(solution)/shard_map/triangular_solve | solution.py:79
  255.9 1.9 bitcast_multiply_fusion.4
  257.9 1.6 fusion.32
  259.5 4.3 convolution_bitcast_fusion
  263.7 4.4 bitcast_subtract_fusion
  268.1 21.8 %while.39 = (s32[]{:T(128)}, f32[3,128,128]{2,1,0:T(8,128)S(1)}, f32[3,128,128]{2,1,0:T(8,128)S(1)}, f32[8,3,128,128]{3,2,0,1:T(8,128)}, f32[8,3,128,128]{3,2,0,1:T(8,128)}, /*index=5*/s32[]{:T(128)}, s32[]{:T(128)}) while((s32[]{:T(128)}, f32[3,128,128]{2,1,0:T(8,128)S(1)}, f32[3,128,128]{2,1,0:T(8,128)S(1)}, ...), condition=%wide.region_3.4_spmd.clone, body=%wide.region_2.3_spmd.clone.sunk | while | flops 151093248 | bytes 2164311 | solution.py:159
  268.2 1.4 convolution_add_fusion.9
  269.6 1.3 fusion.149
  270.9 1.4 convolution_add_fusion.9
  272.3 1.3 fusion.149
  273.7 1.4 convolution_add_fusion.9
  275.1 1.3 fusion.149
  276.4 1.4 convolution_add_fusion.9
  277.8 1.3 fusion.149
  279.1 1.4 convolution_add_fusion.9
  280.5 1.3 fusion.149
  281.8 1.4 convolution_add_fusion.9
  283.2 1.3 fusion.149
  284.5 1.4 convolution_add_fusion.9
  285.9 1.3 fusion.149
  287.3 1.4 convolution_add_fusion.9
  288.7 1.3 fusion.149
  290.6 1.3 reshape.193
  291.9 1.9 fusion.54
  296.5 1.5 fusion.57
  298.9 1.6 copy.85
  300.5 2.5 fusion.56
  304.0 1.4 slice_bitcast_fusion.1
  306.4 2.3 fusion.36
  308.7 32.3 %all-gather = bf16[24,128,128]{2,1,0:T(8,128)(2,1)S(1)} all-gather(bf16[3,128,128]{2,1,0:T(8,128)(2,1)S(1)} %convert_element_type.86), channel_id=2, replica_groups=mesh['ep'=8,'tp'=4] {'ep'}, dimensions={0}, use_global_device_ids=true | all-gather | bytes 884736 | tf_op jit(solution)/shard_map/all_gather | solution.py:13
  341.0 34.0 %all-gather.1 = bf16[24,128,128]{2,1,0:T(8,128)(2,1)} all-gather(bf16[3,128,128]{2,1,0:T(8,128)(2,1)S(1)} %copy-done.8), channel_id=3, replica_groups=mesh['ep'=8,'tp'=4] {'ep'}, dimensions={0}, use_global_device_ids=true | all-gather | bytes 884736 | tf_op jit(solution)/shard_map/all_gather | solution.py:13
  375.1 2.6 fusion.99
  377.6 5.8 %convolution_convert_fusion.1 = bf16[512,2048]{1,0:T(8,128)(2,1)} fusion(bf16[256,2048]{1,0:T(8,128)(2,1)} %param.43, bf16[512,2048]{1,0:T(8,128)(2,1)} %all-gather.5.cloned.1.call-done, bf16[2048,256]{1,0:T(8,128)(2,1)} %param.42, f32[512,256]{1,0:T(8,128)S(1)} %fusion.99), kind=kOutput, calls=%fused_computation.41 | convolution fusion | flops 1075576832 | bytes 6815744 | tf_op jit(solution)/shard_map/dot_general | solution.py:294
  384.6 38.8 %while.38 = (s32[]{:T(128)}, f32[3,128,128]{2,1,0:T(8,128)S(1)}, f32[8,3,64,128]{3,2,1,0:T(8,128)S(1)}, f32[8,3]{1,0:T(8,128)}, f32[8,3,64,128]{3,2,1,0:T(8,128)...) while((s32[]{:T(128)}, f32[3,128,128]{2,1,0:T(8,128)S(1)}, ...), condition=%wide.region_8.9_spmd, body=%wide.region_7.8_spmd.sunk | while | flops 132268032 | bytes 1870981 | solution.py:170
  384.6 1.2 convolution_subtract_fusion.2
  385.8 1.2 fusion.143
  389.4 1.2 convolution_subtract_fusion.2
  394.3 1.2 convolution_subtract_fusion.2
  395.5 1.2 fusion.143
  399.1 1.3 convolution_subtract_fusion.2
  400.4 1.2 fusion.143
  404.0 1.2 convolution_subtract_fusion.2
  408.9 1.2 convolution_subtract_fusion.2
  413.7 1.2 convolution_subtract_fusion.2
  415.0 1.2 fusion.143
  418.5 1.2 convolution_subtract_fusion.2
  424.3 2.6 convolution_convert_fusion.2
  427.0 13.9 %all-to-all-start.1 = ((bf16[8,48,2048]{2,1,0:T(8,128)(2,1)}), bf16[8,48,2048]{2,1,0:T(8,128)(2,1)S(1)}, u32[]{:S(2)}, u32[]{:S(2)}) async-start(bf16[8,48,2048]{2,1,0:T(8,128)(2,1)} %bitcast.235), calls=%async_computation.4 | async-start | bytes 3145728 | tf_op jit(solution)/shard_map/all_to_all | solution.py:282
  441.0 25.7 %all-to-all-done.1 = bf16[8,48,2048]{2,1,0:T(8,128)(2,1)S(1)} async-done(((bf16[8,48,2048]{2,1,0:T(8,128)(2,1)}), bf16[8,48,2048]{2,1,0:T(8,128)(2,1)S(1)}, u32[]{:S(2)}, u32[]{:S(2)}) %all-to-all-start.1) | async-done | bytes 1572896 | tf_op jit(solution)/shard_map/all_to_all | solution.py:282
  466.7 2.3 gather_fusion.1
  469.1 1.7 reshape.186
  470.8 2.5 fusion.98
  473.3 3.6 fusion.47
  (158 shorter events, 39.8 us)
Async XLA Ops:
  7.2 417.2 %copy-start = (bf16[384,2048]{1,0:T(8,128)(2,1)S(1)}, bf16[384,2048]{1,0:T(8,128)(2,1)}, u32[]{:S(2)}) copy-start(bf16[384,2048]{1,0:T(8,128)(2,1)} %param.33) | copy-start | bytes 4718596
  7.2 102.2 %all-gather.7.cloned.1.call-start = ((), (), s32[]{:S(2)}) async-start(), calls=%async_computation.8 | async-start | bytes 7864320 | tf_op jit(solution)/shard_map/all_gather | solution.py:270
  10.3 0.6 copy-start.14
  14.9 3.2 copy-start.1
  63.9 45.5 %copy-start.18 = (bf16[1,2048,256]{2,1,0:T(8,128)(2,1)S(1)}, bf16[1,2048,256]{2,1,0:T(8,128)(2,1)}, u32[]{:S(2)}) copy-start(bf16[1,2048,256]{2,1,0:T(8,128)(2,1)} %param.38) | copy-start | bytes 3145732
  63.9 311.2 %all-gather.5.cloned.1.call-start = ((), (), s32[]{:S(2)}) async-start(), calls=%async_computation.6 | async-start | bytes 2621440 | tf_op jit(solution)/shard_map/all_gather | solution.py:291
  64.6 362.4 %reduce-scatter.8.cloned.1.call-start = ((), (), s32[]{:S(2)}) async-start(), calls=%async_computation.9 | async-start | bytes 7864320 | tf_op jit(solution)/shard_map/reduce_scatter | solution.py:274
  128.4 1.0 copy-start.9
  128.4 1.3 copy-start.11
  128.4 1.4 copy-start.12
  128.4 1.5 copy-start.19
  128.4 1.5 copy-start.13
  128.4 344.9 %reduce-scatter.6.cloned.1.call-start = ((), (), s32[]{:S(2)}) async-start(), calls=%async_computation.7 | async-start | bytes 2621440 | tf_op jit(solution)/shard_map/reduce_scatter | solution.py:293
  255.9 1.9 copy-start.7
  259.4 4.3 copy-start.3
  268.1 22.5 %copy-start.10 = (bf16[512,384]{1,0:T(8,128)(2,1)S(1)}, bf16[512,384]{1,0:T(8,128)(2,1)}, u32[]{:S(2)}) copy-start(bf16[512,384]{1,0:T(8,128)(2,1)} %param.25) | copy-start | bytes 1179652
  300.5 3.5 copy-start.4
  304.0 1.4 copy-start.2
  304.0 1.7 copy-start.6
  306.3 34.6 %copy-start.8 = (bf16[3,128,128]{2,1,0:T(8,128)(2,1)S(1)}, bf16[3,128,128]{2,1,0:T(8,128)(2,1)}, u32[]{:S(2)}) copy-start(bf16[3,128,128]{2,1,0:T(8,128)(2,1)} %convert_element_type.87) | copy-start | bytes 294916
  383.4 1.1 copy-start.5
  383.5 93.4 %reduce-scatter.4.cloned.1.call-start = ((), (), s32[]{:S(2)}) async-start(), calls=%async_computation.5 | async-start | bytes 2621440 | tf_op jit(solution)/shard_map/reduce_scatter | solution.py:251
  384.6 39.1 %copy-start.17 = (f32[128]{0:T(128)S(1)}, f32[128]{0:T(128)}, u32[]{:S(2)}) copy-start(f32[128]{0:T(128)} %param.32) | copy-start | bytes 1540
  427.0 13.9 %copy-start.15 = (s32[256,1]{0,1:T(1,128)S(1)}, s32[256,1]{0,1:T(1,128)}, u32[]{:S(2)}) copy-start(s32[256,1]{0,1:T(1,128)} %copy-done.14) | copy-start | bytes 3076
  427.0 13.9 %copy-start.16 = (f32[128,2]{0,1:T(2,128)S(1)}, f32[128,2]{0,1:T(2,128)}, u32[]{:S(2)}) copy-start(f32[128,2]{0,1:T(2,128)} %param.37) | copy-start | bytes 3076
  427.0 39.7 %all-to-all-start.1 = ((bf16[8,48,2048]{2,1,0:T(8,128)(2,1)}), bf16[8,48,2048]{2,1,0:T(8,128)(2,1)S(1)}, u32[]{:S(2)}, u32[]{:S(2)}) async-start(bf16[8,48,2048]{2,1,0:T(8,128)(2,1)} %bitcast.235), calls=%async_computation.4 | async-start | bytes 3145728 | tf_op jit(solution)/shard_map/all_to_all | solution.py:282
Sparse Core Ops, SparseCore 0:
  64.0 45.3 all-gather.6
  111.5 22.5 all-gather.4
  136.7 59.0 reduce-scatter.7
  383.6 39.5 reduce-scatter.5
  427.1 39.5 reduce-scatter.3
where the time goes:
time: 486 us; the launch traced here: 483 us
  other arithmetic  140 us (29%)
  blocking collectives  110 us (23%)
  matrix products  99.6 us (20%)
  waiting for transfers between devices  71.3 us (15%)
  local copies, waits for them, and re-layouts  33 us (7%)
  between operations  14.2 us (3%)
  starting transfers between devices  14.1 us (3%)
    another operation x3, other arithmetic, block_contributions(): lax.linalg.triangular_solve(lower_part, right_side, left_side=True, lower...  119 us
    all_gather x2, blocking collectives, prefix_2(): lax.all_gather(a.astype(kind), axis)  66.3 us
    all_gather x1, waiting for transfers between devices, shards(): lax.all_gather(arrived, 'tp', axis=0, tiled=True)  44.7 us
    all_to_all x1, blocking collectives, shards(): lax.all_to_all(outgoing, 'ep', split_axis=0, concat_axis=0, tiled=True)  44.2 us
    all_to_all x1, waiting for transfers between devices, shards(): lax.all_to_all(slot_sums.reshape(experts, capacity, model_width), 'ep', s...  25.7 us
    dot_general x16, matrix products, mat_product(): return jnp.einsum('hde,hef->hdf', left_mat, right_mat, precision=HIGH)  21.2 us
    all_to_all x1, starting transfers between devices, shards(): lax.all_to_all(slot_sums.reshape(experts, capacity, model_width), 'ep', s...  13.9 us
    dot_general x1, matrix products, shards(): jnp.dot(hidden, routed_down_weight[0], preferred_element_type=jnp.float32)  13.2 us
  transfers between devices with their start and end apart: 6, of which 2 were waited for; matrix products, arithmetic and copies ran while one was open for 53% of the time, Pallas kernels for 0%

commit v1 on v0

v1 whole, which is shorter than its diff:
```python
import jax
import jax.numpy as jnp
from jax import lax
from jax.experimental import pallas as pl
from jax.experimental.pallas import tpu as pltpu
from jax.sharding import PartitionSpec as P


EPS = 1e-06


SPAN = 64


def halves(x):
    high = x.astype(jnp.bfloat16)
    return high, (x - high.astype(jnp.float32)).astype(jnp.bfloat16)


def product(left, right, numbers):
    left_high, left_low = halves(left)
    right_high, right_low = halves(right)

    def dot(x, y):
        return lax.dot_general(x, y, numbers, preferred_element_type=jnp.float32)

    return dot(left_high, right_high) + (dot(left_high, right_low) + dot(left_low, right_high))


def bmm(left, right, dims):
    return product(left, right, (dims, ((0,), (0,))))


def mm(left, right):
    return product(left, right, (((1,), (0,)), ((), ())))


def unit_lower_inverse(lower, rows, cols):
    inverse = jnp.where(rows == cols, 1.0, 0.0) - jnp.where(
        ((rows >> 1) == (cols >> 1)), lower, 0.0
    )
    level = 1
    while (1 << level) < SPAN:
        below = ((rows >> (level + 1)) == (cols >> (level + 1))) & (
            (rows >> level) != (cols >> level)
        )
        part = jnp.where(below, lower, 0.0)
        inverse = inverse - bmm(bmm(inverse, part, ((2,), (1,))), inverse, ((2,), (1,)))
        level += 1
    return inverse


def local_kernel(q_ref, k_ref, v_ref, ccol_ref, crow_ref, bcol_ref, g_ref, z_ref, total_ref):
    width = q_ref.shape[1]
    count = q_ref.shape[0] // SPAN
    shape = (count, SPAN, width)
    q = q_ref[...].astype(jnp.float32)
    k = k_ref[...].astype(jnp.float32)
    v = v_ref[...].astype(jnp.float32).reshape(shape)
    q = q * lax.rsqrt(jnp.sum(q * q, axis=-1, keepdims=True) + EPS) * width ** (-0.5)
    k = k * lax.rsqrt(jnp.sum(k * k, axis=-1, keepdims=True) + EPS)
    q = q.reshape(shape)
    k = k.reshape(shape)
    ccol = ccol_ref[0].reshape(count, SPAN, 1)
    crow = crow_ref[0]
    bcol = bcol_ref[0].reshape(count, SPAN, 1)
    rows = lax.broadcasted_iota(jnp.int32, (count, SPAN, SPAN), 1)
    cols = lax.broadcasted_iota(jnp.int32, (count, SPAN, SPAN), 2)
    decay = jnp.exp(jnp.where(rows >= cols, ccol - crow, -jnp.inf))
    keyed = k * bcol
    lower = jnp.where(rows > cols, bmm(keyed, k, ((2,), (2,))) * decay, 0.0)
    inverse = unit_lower_inverse(lower, rows, cols)
    grown = jnp.exp(ccol)
    solved = bmm(
        inverse, jnp.concatenate([keyed * grown, v * bcol], axis=-1), ((2,), (1,))
    )
    scores = bmm(q, k, ((2,), (2,))) * decay
    q_scaled = q * grown
    last = ccol[:, SPAN - 1 :, :]
    carried = k * jnp.exp(last - ccol)
    mixed = bmm(scores, solved, ((2,), (1,)))
    readout = q_scaled - mixed[:, :, :width]
    eye_r = lax.broadcasted_iota(jnp.int32, (width, width), 0)
    eye_c = lax.broadcasted_iota(jnp.int32, (width, width), 1)
    eye = jnp.where(eye_r == eye_c, 1.0, 0.0)
    state = jnp.concatenate([eye, jnp.zeros_like(eye)], axis=1)
    for n in range(count):
        seen = mm(readout[n], state)
        g_ref[0, n * SPAN : (n + 1) * SPAN, :] = seen[:, :width]
        z_ref[0, n * SPAN : (n + 1) * SPAN, :] = seen[:, width:] + mixed[n][:, width:]
        both = mm(carried[n].T, solved[n])
        trans = jnp.exp(last[n]) * eye - both[:, :width]
        state = mm(trans, state)
        state = jnp.concatenate([state[:, :width], state[:, width:] + both[:, width:]], axis=1)
    total_ref[0] = state.astype(jnp.bfloat16)


def finish_kernel(place_ref, gathered_ref, g_ref, z_ref, gain_ref, out_ref):
    width = g_ref.shape[2]

    def one(turn, state):
        both = gathered_ref[turn, 0].astype(jnp.float32)
        return mm(both[:, :width], state) + both[:, width:]

    state = lax.fori_loop(0, place_ref[0], one, jnp.zeros((width, width), jnp.float32))
    out = mm(g_ref[0], state) + z_ref[0]
    out = out * lax.rsqrt(jnp.mean(out * out, axis=-1, keepdims=True) + EPS) * gain_ref[...]
    out_ref[...] = out.astype(jnp.bfloat16)


def token_mixer_heads(
    queries,
    keys,
    values,
    decay_gate_logits,
    correction_logits,
    head_decay_speed,
    position_log_decay,
    head_output_gain,
):
    heads = decay_gate_logits.shape[1]
    length = queries.shape[0]
    width = queries.shape[1] // heads
    count = length // SPAN
    log_gate = -head_decay_speed * jax.nn.softplus(decay_gate_logits) + position_log_decay
    log_gate = log_gate.T.reshape(heads, count, SPAN)
    at = jnp.arange(SPAN)
    cum = jnp.sum(
        jnp.where(at[:, None] >= at[None, :], log_gate[:, :, None, :], 0.0), axis=-1
    )
    beta = jax.nn.sigmoid(correction_logits.astype(jnp.float32)).T.reshape(heads, length, 1)
    by_head = pl.BlockSpec((length, width), lambda h: (0, h))
    column = pl.BlockSpec((1, length, 1), lambda h: (h, 0, 0))
    whole = pl.BlockSpec((1, length, width), lambda h: (h, 0, 0))
    local_call = pl.pallas_call(
        local_kernel,
        grid=(heads,),
        in_specs=[
            by_head,
            by_head,
            by_head,
            column,
            pl.BlockSpec((1, count, 1, SPAN), lambda h: (h, 0, 0, 0)),
            column,
        ],
        out_specs=[whole, whole, pl.BlockSpec((1, width, 2 * width), lambda h: (h, 0, 0))],
        out_shape=[
            jax.ShapeDtypeStruct((heads, length, width), jnp.float32),
            jax.ShapeDtypeStruct((heads, length, width), jnp.float32),
            jax.ShapeDtypeStruct((heads, width, 2 * width), jnp.bfloat16),
        ],
        cost_estimate=pl.CostEstimate(
            flops=3_000_000_000, bytes_accessed=4_000_000, transcendentals=200_000
        ),
    )
    readout, local_out, total = local_call(
        queries,
        keys,
        values,
        cum.reshape(heads, length, 1),
        cum.reshape(heads, count, 1, SPAN),
        beta,
    )
    gathered = lax.all_gather(total, "ep")
    place = lax.axis_index("ep").astype(jnp.int32).reshape(1)
    devices = gathered.shape[0]
    return pl.pallas_call(
        finish_kernel,
        grid=(heads,),
        in_specs=[
            pl.BlockSpec(memory_space=pltpu.SMEM),
            pl.BlockSpec((devices, 1, width, 2 * width), lambda h: (0, h, 0, 0)),
            whole,
            whole,
            pl.BlockSpec((1, width), lambda h: (0, 0)),
        ],
        out_specs=by_head,
        out_shape=jax.ShapeDtypeStruct((length, heads * width), jnp.bfloat16),
        cost_estimate=pl.CostEstimate(
            flops=500_000_000, bytes_accessed=4_000_000, transcendentals=2_000
        ),
    )(place, gathered, readout, local_out, head_output_gain.reshape(1, width))


def norm_rows(expert_input_tokens, expert_norm_gain):
    rows_f = expert_input_tokens.astype(jnp.float32)
    scaled = (
        rows_f
        * lax.rsqrt(jnp.mean(rows_f * rows_f, axis=-1, keepdims=True) + EPS)
        * expert_norm_gain
    )
    return scaled.astype(jnp.bfloat16)


def gated_hidden(rows_in, w_gate, w_up):
    gate_val = jnp.dot(rows_in, w_gate, preferred_element_type=jnp.float32)
    up_val = jnp.dot(rows_in, w_up, preferred_element_type=jnp.float32)
    return (jax.nn.silu(gate_val) * up_val).astype(jnp.bfloat16)


def slot_layout(routes, capacity):
    flat = routes.reshape(-1)
    at = jnp.arange(flat.shape[0], dtype=jnp.int32)
    same = (flat[:, None] == flat[None, :]) & (at[None, :] < at[:, None])
    before = jnp.sum(same.astype(jnp.int32), axis=1)
    return (flat * capacity + before).reshape(routes.shape)


def shards(
    queries,
    keys,
    values,
    decay_gate_logits,
    correction_logits,
    head_decay_speed,
    position_log_decay,
    head_output_gain,
    mixer_output_weight,
    expert_input_tokens,
    expert_norm_gain,
    routes,
    chosen_expert_weight,
    routed_gate_weight,
    routed_up_weight,
    routed_down_weight,
    common_gate_weight,
    common_up_weight,
    common_down_weight,
):
    normed = token_mixer_heads(
        queries,
        keys,
        values,
        decay_gate_logits,
        correction_logits,
        head_decay_speed,
        position_log_decay,
        head_output_gain,
    )
    mixer_out = lax.psum_scatter(
        jnp.dot(normed, mixer_output_weight, preferred_element_type=jnp.float32).astype(
            jnp.bfloat16
        ),
        "tp",
        scatter_dimension=0,
        tiled=True,
    )
    normed_in = norm_rows(expert_input_tokens, expert_norm_gain)
    tokens_own, top_k = routes.shape
    model_width = expert_input_tokens.shape[1]
    experts = lax.axis_size("ep")
    capacity = 3 * tokens_own * top_k // (2 * experts)
    slot_count = experts * capacity
    slots = slot_layout(routes, capacity)
    numbers = jnp.arange(slot_count, dtype=jnp.int32)
    sends = sum(
        (slots[None, :, k] == numbers[:, None]).astype(jnp.bfloat16) for k in range(top_k)
    )
    outgoing = jnp.dot(sends, normed_in, preferred_element_type=jnp.float32).astype(
        jnp.bfloat16
    )
    arrived = lax.all_to_all(
        outgoing.reshape(experts, capacity, model_width),
        "ep",
        split_axis=0,
        concat_axis=0,
        tiled=True,
    ).reshape(slot_count, model_width)
    gate_all = lax.all_gather(routed_gate_weight[0], "tp")
    up_all = lax.all_gather(routed_up_weight[0], "tp")
    down_all = lax.all_gather(routed_down_weight[0], "tp", axis=0, tiled=True)
    hidden = jnp.concatenate(
        [gated_hidden(arrived, gate_all[t], up_all[t]) for t in range(gate_all.shape[0])],
        axis=1,
    )
    slot_sums = jnp.dot(hidden, down_all, preferred_element_type=jnp.float32).astype(
        jnp.bfloat16
    )
    returned = lax.all_to_all(
        slot_sums.reshape(experts, capacity, model_width),
        "ep",
        split_axis=0,
        concat_axis=0,
        tiled=True,
    ).reshape(slot_count, model_width)
    shared_hidden = gated_hidden(
        lax.all_gather(normed_in, "tp", axis=0, tiled=True), common_gate_weight, common_up_weight
    )
    shared = lax.psum_scatter(
        jnp.dot(shared_hidden, common_down_weight, preferred_element_type=jnp.float32).astype(
            jnp.bfloat16
        ),
        "tp",
        scatter_dimension=0,
        tiled=True,
    ).astype(jnp.float32)
    weights = sum(
        jnp.where(
            slots[:, k : k + 1] == numbers[None, :], chosen_expert_weight[:, k : k + 1], 0.0
        )
        for k in range(top_k)
    )
    coarse = weights.astype(jnp.bfloat16)
    fine = (weights - coarse.astype(jnp.float32)).astype(jnp.bfloat16)
    routed = jnp.dot(coarse, returned, preferred_element_type=jnp.float32) + jnp.dot(
        fine, returned, preferred_element_type=jnp.float32
    )
    moe_out = (shared + routed).astype(jnp.bfloat16)
    return (mixer_out, moe_out)


def solution(mesh):
    return jax.shard_map(
        shards,
        mesh=mesh,
        in_specs=(
            P("ep", "tp"),
            P("ep", "tp"),
            P("ep", "tp"),
            P("ep", "tp"),
            P("ep", "tp"),
            P("tp"),
            P("ep", "tp"),
            P(),
            P("tp", None),
            P(("ep", "tp"), None),
            P(),
            P(("ep", "tp"), None),
            P(("ep", "tp"), None),
            P("ep", None, "tp"),
            P("ep", None, "tp"),
            P("ep", "tp", None),
            P(None, "tp"),
            P(None, "tp"),
            P("tp", None),
        ),
        out_specs=(P(("ep", "tp"), None), P(("ep", "tp"), None)),
        check_vma=False,
    )
```

time: 486 us -> 285 us (0.59)
  other arithmetic: 140 us -> 3.93 us
  waiting for transfers between devices: 71.3 us -> 187 us
  blocking collectives: 110 us -> 0 us
  matrix products: 99.6 us -> 39.6 us
  local copies, waits for them, and re-layouts: 33 us -> 4.13 us
  Pallas kernels: 0 us -> 22.7 us
    another operation x6 -> x0, other arithmetic: 121 us -> none  [the longest x3 119 us: block_contributions(): lax.linalg.triangular_solve(lower_part, right_side, left_side=True, lower...]
    all_gather x1 -> x4, waiting for transfers between devices: 44.7 us -> 132 us  [the longest x1 50.2 us: token_mixer_heads(): gathered = lax.all_gather(total, 'ep')]
    all_gather x2 -> x0, blocking collectives: 66.3 us -> none  [prefix_2(): lax.all_gather(a.astype(kind), axis)]
    dot_general x53 -> x8, matrix products: 81.3 us -> 18.6 us  [the longest x4 7.24 us: gated_hidden(): up_val = jnp.dot(rows_in, w_up, preferred_element_type=jnp.float32)]
    all_to_all x1 -> x0, blocking collectives: 44.2 us -> none  [shards(): lax.all_to_all(outgoing, 'ep', split_axis=0, concat_axis=0, tiled=True)]
    pallas_call x0 -> x2, Pallas kernels: none -> 22.7 us  [the longest x1 18.9 us: token_mixer_heads(): local_call(queries, keys, values, cum.reshape(heads, length, 1), cum.resh...]
    reduce_scatter x1, waiting for transfers between devices: 0.01 us -> 15.2 us  [shards(): lax.psum_scatter(jnp.dot(normed, mixer_output_weight, preferred_element_t...]
    all_to_all x1, waiting for transfers between devices: 25.7 us -> 37.4 us  [shards(): lax.all_to_all(slot_sums.reshape(experts, capacity, model_width), 'ep', s...]
  transfers between devices with their start and end apart: 6 -> 9, of which waited for: 2 -> 7; matrix products, arithmetic and copies ran while one was open for 53% -> 15% of each run, Pallas kernels for 0% -> 8%
where the time goes in v1:
time: 285 us; the launch traced here: 284 us
  waiting for transfers between devices  187 us (66%)
  matrix products  39.6 us (14%)
  Pallas kernels  22.7 us (8%)
  between operations  14.3 us (5%)
  starting transfers between devices  12.3 us (4%)
  local copies, waits for them, and re-layouts  4.13 us (1%)
  other arithmetic  3.93 us (1%)
    all_gather x1, waiting for transfers between devices, token_mixer_heads(): gathered = lax.all_gather(total, 'ep')  50.2 us
    all_to_all x1, waiting for transfers between devices, shards(): lax.all_to_all(slot_sums.reshape(experts, capacity, model_width), 'ep', s...  37.4 us
    all_gather x1, waiting for transfers between devices, shards(): up_all = lax.all_gather(routed_up_weight[0], 'tp')  28.5 us
    all_gather x1, waiting for transfers between devices, shards(): down_all = lax.all_gather(routed_down_weight[0], 'tp', axis=0, tiled=True)  26.7 us
    all_gather x1, waiting for transfers between devices, shards(): gate_all = lax.all_gather(routed_gate_weight[0], 'tp')  26.5 us
    pallas_call x1, Pallas kernels, token_mixer_heads(): local_call(queries, keys, values, cum.reshape(heads, length, 1), cum.resh...  18.9 us
    reduce_scatter x1, waiting for transfers between devices, shards(): lax.psum_scatter(jnp.dot(normed, mixer_output_weight, preferred_element_t...  15.2 us
    dot_general x5, matrix products, gated_hidden(): gate_val = jnp.dot(rows_in, w_gate, preferred_element_type=jnp.float32)  11.7 us
  transfers between devices with their start and end apart: 9, of which 7 were waited for; matrix products, arithmetic and copies ran while one was open for 15% of the time, Pallas kernels for 8%

profile of v1, /device:TPU:0, one launch (start us, length us, event | category | flops | bytes accessed | tf_op | source)
XLA Modules:
  0.0 284.4 jit_solution(4751958373943976979)
XLA Ops:
  7.2 0.0 copy-start
  7.2 0.0 copy-start.10
  7.2 0.0 copy-start.4
  7.2 0.0 copy-start.3
  7.2 0.0 copy-start.6
  7.2 0.0 all-gather.8.cloned.1.call-start
  7.3 1.3 fusion.12
  8.6 2.0 fusion.14
  10.6 0.0 all-gather.8.cloned.1.call-update
  10.7 0.0 all-gather.14.cloned.1.call-start
  10.7 0.0 copy-done.4
  10.7 0.0 copy-done.3
  10.8 0.1 fusion.51
  10.8 0.1 broadcast_in_dim.52
  10.9 0.3 select_reduce_fusion
  11.2 1.6 reshape.60.ccol_ref
  12.9 1.2 copy.43.bcol_ref
  14.1 18.9 %shard_map.194 = (f32[3,512,128]{2,1,0:T(8,128)}, f32[3,512,128]{2,1,0:T(8,128)}, bf16[3,128,256]{2,1,0:T(8,128)(2,1)}) custom-call(bf16[512,384]{1,0:T(8,128)(2,1)} %q_ref.1, bf16[512,384]{1,0:T(8,128)(2,1)} %k_ref.1, bf16[512,384]{1,0:T(8,128)(2,1)} %v_ref.1, f32[3,512,1]{2,1,0:T(8,128)} %reshape.60.ccol_ref, f32[3,8,1,64]{3,2,1,0:T(1,128)} %bitcast.81, ...), custom_call_target="tpu_custom_call" | custom-call | flops 3000000000 | bytes 4000000 | tf_op jit(solution)/shard_map/pallas_call | solution.py:156
  33.0 0.0 all-gather.14.cloned.1.call-update
  33.1 0.0 copy-start.9
  33.1 0.0 all-gather.10.cloned.1.call-start
  33.1 0.7 all-gather.10.cloned.1.call-update
  33.8 0.0 all-gather.12.cloned.1.call-start
  33.9 0.5 all-gather.12.cloned.1.call-update
  34.4 0.0 all-gather.16.cloned.1.call-start
  34.4 0.5 all-gather.16.cloned.1.call-update
  35.0 0.0 reduce-scatter.5.cloned.1.call-start
  35.0 1.2 all-gather.8.cloned.1.call-done
  36.2 2.3 fusion.56
  38.5 5.8 %convolution_convert_fusion = bf16[512,2048]{1,0:T(8,128)(2,1)} fusion(bf16[256,2048]{1,0:T(8,128)(2,1)} %param.37, bf16[512,2048]{1,0:T(8,128)(2,1)} %all-gather.8.cloned.1.call-done, bf16[2048,256]{1,0:T(8,128)(2,1)} %param.36, f32[512,256]{1,0:T(8,128)S(1)} %fusion.56), kind=kOutput, calls=%fused_computation.2 | convolution fusion | flops 1075576832 | bytes 6815744 | tf_op jit(solution)/shard_map/dot_general | solution.py:290
  44.3 0.0 reduce-scatter.5.cloned.1.call-update
  44.3 0.7 copy-done.5
  44.9 0.1 copy.44
  45.1 0.1 eq.71
  45.2 0.2 convert_reduce_fusion
  45.4 0.1 reduce_sum.32
  45.5 0.1 copy.45
  45.6 0.0 copy-done.1
  45.6 1.7 convolution_convert_fusion.2
  47.4 6.2 %all-to-all-start = ((bf16[8,48,2048]{2,1,0:T(8,128)(2,1)}), bf16[8,48,2048]{2,1,0:T(8,128)(2,1)S(1)}, u32[]{:S(2)}, u32[]{:S(2)}) async-start(bf16[8,48,2048]{2,1,0:T(8,128)(2,1)} %bitcast.11), calls=%async_computation.2 | async-start | bytes 3145728 | tf_op jit(solution)/shard_map/all_to_all | solution.py:262
  53.6 0.2 reduce-scatter.3.cloned.1.call-start
  53.8 50.2 %all-gather.14.cloned.1.call-done = bf16[24,128,256]{2,1,0:T(8,128)(2,1)} async-done(((bf16[3,128,256]{2,1,0:T(8,128)(2,1)}), bf16[24,128,256]{2,1,0:T(8,128)(2,1)}) %all-gather.14.cloned.1.call-update) | async-done | bytes 1572880 | tf_op jit(solution)/shard_map/all_gather | solution.py:164
  104.0 3.8 %shard_map.195 = bf16[512,384]{1,0:T(8,128)(2,1)} custom-call(s32[1]{0:T(128)} %bitcast.place_ref, bf16[8,3,128,256]{3,2,1,0:T(8,128)(2,1)} %bitcast.80, f32[3,512,128]{2,1,0:T(8,128)} %get-tuple-element.6.g_ref, f32[3,512,128]{2,1,0:T(8,128)} %get-tuple-element.7.z_ref, f32[1,128]{1,0:T(1,128)} %bitcast.82), custom_call_target="tpu_custom_call" | custom-call | flops 500000000 | bytes 4000000 | tf_op jit(solution)/shard_map/pallas_call | solution.py:167
  107.8 3.6 %convolution_convert_fusion.1 = bf16[512,2048]{1,0:T(8,128)(2,1)} fusion(bf16[512,384]{1,0:T(8,128)(2,1)} %shard_map.195, bf16[384,2048]{1,0:T(8,128)(2,1)S(1)} %copy-done), kind=kOutput, calls=%fused_computation.3 | convolution fusion | flops 806354944 | bytes 4063232 | tf_op jit(solution)/shard_map/dot_general | solution.py:241
  111.4 0.0 reduce-scatter.3.cloned.1.call-update
  111.4 0.0 all-to-all-done
  111.4 26.5 %all-gather.10.cloned.1.call-done = bf16[4,2048,256]{2,1,0:T(8,128)(2,1)} async-done(((bf16[1,2048,256]{2,1,0:T(8,128)(2,1)}), bf16[4,2048,256]{2,1,0:T(8,128)(2,1)}) %all-gather.10.cloned.1.call-update) | async-done | bytes 4194320 | tf_op jit(solution)/shard_map/all_gather | solution.py:269
  138.0 2.7 fusion.16
  140.7 2.7 fusion.15
  143.4 2.0 fusion.18
  145.4 28.5 %all-gather.12.cloned.1.call-done = bf16[4,2048,256]{2,1,0:T(8,128)(2,1)} async-done(((bf16[1,2048,256]{2,1,0:T(8,128)(2,1)}), bf16[4,2048,256]{2,1,0:T(8,128)(2,1)}) %all-gather.12.cloned.1.call-update) | async-done | bytes 4194320 | tf_op jit(solution)/shard_map/all_gather | solution.py:270
  173.9 2.9 %fusion.10 = bf16[384,256]{0,1:T(8,128)(2,1)} fusion(bf16[384,2048]{1,0:T(8,128)(2,1)S(1)} %bitcast.74, bf16[4,2048,256]{2,1,0:T(8,128)(2,1)} %all-gather.12.cloned.1.call-done, f32[384,256]{0,1:T(8,128)} %fusion.16), kind=kOutput, calls=%fused_computation.19 | convolution fusion | flops 403243008 | bytes 3211264 | tf_op jit(solution)/shard_map/dot_general | solution.py:197
  176.8 1.4 fusion.11
  178.2 1.4 fusion.8
  179.7 2.0 fusion.17
  181.7 0.0 copy-start.13
  181.7 1.5 fusion.9
  183.1 26.7 %all-gather.16.cloned.1.call-done = bf16[1,1024,2048]{2,1,0:T(8,128)(2,1)} async-done(((bf16[1,256,2048]{2,1,0:T(8,128)(2,1)}), bf16[1,1024,2048]{2,1,0:T(8,128)(2,1)}) %all-gather.16.cloned.1.call-update) | async-done | bytes 4194320 | tf_op jit(solution)/shard_map/all_gather | solution.py:271
  209.8 5.4 %fusion.2 = bf16[384,2048]{1,0:T(8,128)(2,1)} fusion(bf16[1,1024,2048]{2,1,0:T(8,128)(2,1)} %all-gather.16.cloned.1.call-done, bf16[384,256]{0,1:T(8,128)(2,1)S(1)} %copy-done.13, bf16[384,256]{0,1:T(8,128)(2,1)S(1)} %copy-done.12, bf16[384,256]{0,1:T(8,128)(2,1)} %fusion.9, bf16[384,256]{0,1:T(8,128)(2,1)} %fusion.8), kind=kOutput, calls=%fused_computation.4 | convolution fusion | flops 1614544896 | bytes 6553600 | tf_op jit(solution)/shard_map/dot_general | solution.py:276
  215.2 5.6 %all-to-all-start.1 = ((bf16[8,48,2048]{2,1,0:T(8,128)(2,1)}), bf16[8,48,2048]{2,1,0:T(8,128)(2,1)S(1)}, u32[]{:S(2)}, u32[]{:S(2)}) async-start(bf16[8,48,2048]{2,1,0:T(8,128)(2,1)} %bitcast.79), calls=%async_computation.3 | async-start | bytes 3145728 | tf_op jit(solution)/shard_map/all_to_all | solution.py:279
  220.8 37.4 %all-to-all-done.1 = bf16[8,48,2048]{2,1,0:T(8,128)(2,1)S(1)} async-done(((bf16[8,48,2048]{2,1,0:T(8,128)(2,1)}), bf16[8,48,2048]{2,1,0:T(8,128)(2,1)S(1)}, u32[]{:S(2)}, u32[]{:S(2)}) %all-to-all-start.1) | async-done | bytes 1572896 | tf_op jit(solution)/shard_map/all_to_all | solution.py:279
  258.2 1.5 fusion.47
  259.8 2.7 fusion.6
  262.4 15.2 %reduce-scatter.3.cloned.1.call-done = bf16[128,2048]{1,0:T(8,128)(2,1)} async-done(((bf16[512,2048]{1,0:T(8,128)(2,1)}), bf16[128,2048]{1,0:T(8,128)(2,1)}) %reduce-scatter.3.cloned.1.call-update) | async-done | bytes 524304 | tf_op jit(solution)/shard_map/reduce_scatter | solution.py:240
  (25 shorter events, 0.1 us)
Async XLA Ops:
  7.2 100.6 %copy-start = (bf16[384,2048]{1,0:T(8,128)(2,1)S(1)}, bf16[384,2048]{1,0:T(8,128)(2,1)}, u32[]{:S(2)}) copy-start(bf16[384,2048]{1,0:T(8,128)(2,1)} %param.27) | copy-start | bytes 4718596
  7.2 3.5 %copy-start.10 = (f32[3]{0:T(128)S(1)}, f32[3]{0:T(128)}, u32[]{:S(2)}) copy-start(f32[3]{0:T(128)} %param.24) | copy-start | bytes 40
  7.2 3.5 %copy-start.4 = (f32[512,3]{0,1:T(4,128)S(1)}, f32[512,3]{0,1:T(4,128)}, u32[]{:S(2)}) copy-start(f32[512,3]{0,1:T(4,128)} %param.22) | copy-start | bytes 18436
  7.2 3.5 %copy-start.3 = (f32[512,3]{0,1:T(4,128)S(1)}, f32[512,3]{0,1:T(4,128)}, u32[]{:S(2)}) copy-start(f32[512,3]{0,1:T(4,128)} %param.25) | copy-start | bytes 18436
  7.2 5.6 %copy-start.6 = (bf16[512,3]{0,1:T(4,128)(2,1)S(1)}, bf16[512,3]{0,1:T(4,128)(2,1)}, u32[]{:S(2)}) copy-start(bf16[512,3]{0,1:T(4,128)(2,1)} %param.23) | copy-start | bytes 9220
  7.2 29.0 %all-gather.8.cloned.1.call-start = ((), (), s32[]{:S(2)}) async-start(), calls=%async_computation.5 | async-start | bytes 2621440 | tf_op jit(solution)/shard_map/all_gather | solution.py:287
  10.7 93.3 %all-gather.14.cloned.1.call-start = ((), (), s32[]{:S(2)}) async-start(), calls=%async_computation.9 | async-start | bytes 1769472 | tf_op jit(solution)/shard_map/all_gather | solution.py:164
  11.2 2.9 %copy-start.2 = (f32[3,8,64]{2,1,0:T(8,128)}, f32[3,8,64]{2,1,0:T(8,128)S(1)}, u32[]{:S(2)}) copy-start(f32[3,8,64]{2,1,0:T(8,128)S(1)} %select_reduce_fusion) | copy-start | bytes 18436
  33.1 3.1 %copy-start.9 = (bf16[2048,256]{1,0:T(8,128)(2,1)S(1)}, bf16[2048,256]{1,0:T(8,128)(2,1)}, u32[]{:S(2)}) copy-start(bf16[2048,256]{1,0:T(8,128)(2,1)} %param.35) | copy-start | bytes 3145732
  33.1 104.9 %all-gather.10.cloned.1.call-start = ((), (), s32[]{:S(2)}) async-start(), calls=%async_computation.7 | async-start | bytes 5242880 | tf_op jit(solution)/shard_map/all_gather | solution.py:269
  33.8 140.0 %all-gather.12.cloned.1.call-start = ((), (), s32[]{:S(2)}) async-start(), calls=%async_computation.8 | async-start | bytes 5242880 | tf_op jit(solution)/shard_map/all_gather | solution.py:270
  34.4 175.4 %all-gather.16.cloned.1.call-start = ((), (), s32[]{:S(2)}) async-start(), calls=%async_computation.10 | async-start | bytes 5242880 | tf_op jit(solution)/shard_map/all_gather | solution.py:271
  35.0 224.8 %reduce-scatter.5.cloned.1.call-start = ((), (), s32[]{:S(2)}) async-start(), calls=%async_computation.6 | async-start | bytes 2621440 | tf_op jit(solution)/shard_map/reduce_scatter | solution.py:289
  44.3 0.7 copy-start.5
  44.3 1.4 copy-start.1
  47.4 64.0 %all-to-all-start = ((bf16[8,48,2048]{2,1,0:T(8,128)(2,1)}), bf16[8,48,2048]{2,1,0:T(8,128)(2,1)S(1)}, u32[]{:S(2)}, u32[]{:S(2)}) async-start(bf16[8,48,2048]{2,1,0:T(8,128)(2,1)} %bitcast.11), calls=%async_computation.2 | async-start | bytes 3145728 | tf_op jit(solution)/shard_map/all_to_all | solution.py:262
  53.6 224.0 %reduce-scatter.3.cloned.1.call-start = ((), (), s32[]{:S(2)}) async-start(), calls=%async_computation.4 | async-start | bytes 2621440 | tf_op jit(solution)/shard_map/reduce_scatter | solution.py:240
  173.9 2.9 %copy-start.8 = (bf16[4,2048,256]{2,1,0:T(8,128)(2,1)S(1)}, bf16[4,2048,256]{2,1,0:T(8,128)(2,1)}, u32[]{:S(2)}) copy-start(bf16[4,2048,256]{2,1,0:T(8,128)(2,1)} %all-gather.12.cloned.1.call-done) | copy-start | bytes 12582916
  173.9 2.9 %copy-start.11 = (f32[384,256]{0,1:T(8,128)S(1)}, f32[384,256]{0,1:T(8,128)}, u32[]{:S(2)}) copy-start(f32[384,256]{0,1:T(8,128)} %fusion.15) | copy-start | bytes 1179652
  181.6 28.1 %copy-start.12 = (bf16[384,256]{0,1:T(8,128)(2,1)S(1)}, bf16[384,256]{0,1:T(8,128)(2,1)}, u32[]{:S(2)}) copy-start(bf16[384,256]{0,1:T(8,128)(2,1)} %fusion.10) | copy-start | bytes 589828
  181.7 28.1 %copy-start.13 = (bf16[384,256]{0,1:T(8,128)(2,1)S(1)}, bf16[384,256]{0,1:T(8,128)(2,1)}, u32[]{:S(2)}) copy-start(bf16[384,256]{0,1:T(8,128)(2,1)} %fusion.11) | copy-start | bytes 589828
  215.2 5.6 %copy-start.7 = (f32[128,2]{0,1:T(2,128)S(1)}, f32[128,2]{0,1:T(2,128)}, u32[]{:S(2)}) copy-start(f32[128,2]{0,1:T(2,128)} %param.31) | copy-start | bytes 3076
  215.2 43.0 %all-to-all-start.1 = ((bf16[8,48,2048]{2,1,0:T(8,128)(2,1)}), bf16[8,48,2048]{2,1,0:T(8,128)(2,1)S(1)}, u32[]{:S(2)}, u32[]{:S(2)}) async-start(bf16[8,48,2048]{2,1,0:T(8,128)(2,1)} %bitcast.79), calls=%async_computation.3 | async-start | bytes 3145728 | tf_op jit(solution)/shard_map/all_to_all | solution.py:279
Sparse Core Ops, SparseCore 0:
  10.8 25.3 all-gather.7
  38.9 65.0 all-gather.13
  105.6 32.3 all-gather.9
  139.4 34.4 all-gather.11
  175.3 34.4 all-gather.15
  212.2 31.1 reduce-scatter.4
  246.4 31.1 reduce-scatter.2
